TPU v7x, 32 devices: a whole 2x2x4 slice. The times are simulated.
32 devices in a mesh: grp: 2 (over y), ra: 4 (over z), cb: 2 (over x), dp: 2 (over core).
Axes of the slice: x: 2, y: 2, z: 4, core: 2. Of those that a mesh axis runs over, the one named last changes fastest.
Arguments:
- tokens: bfloat16 [256, 2048], P(('grp', 'dp'), 'ra'), parts along dimension 0, may hold values from -62 to 62
- gain_first: float32 [2048], P('ra'), may hold values from 0.1 to 1.9
- up_first: bfloat16 [2048, 8192], P('ra', 'cb'), may hold values from -0.125 to 0.125
- down_first: bfloat16 [8192, 2048], P('cb', 'ra'), may hold values from -0.0625 to 0.0625
- gain_second: float32 [2048], P('ra'), may hold values from 0.1 to 1.9
- up_second: bfloat16 [2048, 8192], P('ra', 'cb'), may hold values from -0.125 to 0.125
- down_second: bfloat16 [8192, 2048], P('cb', 'ra'), may hold values from -0.0625 to 0.0625
- gain_last: float32 [2048], P('ra'), may hold values from 0.1 to 1.9
Outputs:
- normed: bfloat16 [256, 2048], P(('grp', 'dp'), 'ra'), parts along dimension 0
There are 2 independent parts, one for each index of `grp`. A program takes and returns all parts, laid end to end along the dimension named above; an argument that names none is the same for every part. Nothing has to cross between parts.
All inputs are finite; a program needn't handle non-finite values.
Results may differ from a plain program's by a relative error of at most 0.0095.
Values may be sent and summed in bfloat16 or wider, within the bound.
A program may use at most 64 MiB of HBM per device.

v0:
```python
import functools

import jax
import jax.numpy as jnp
from jax import lax
from jax.experimental import pallas as pl
from jax.experimental.pallas import tpu as pltpu
from jax.sharding import PartitionSpec as P

EPS = 1e-06
MESH = pl.DeviceIdType.MESH
F32, BF16 = jnp.float32, jnp.bfloat16

CHUNK = 1024
SPLITS = 4
LAG = 5
SLACK = 3


def kernel(
    n,
    ncb,
    width,
    tokens_ref,
    gain_first,
    up_first,
    down_first,
    gain_second,
    up_second,
    down_second,
    gain_last,
    out_ref,
    tokens_v,
    gain_v,
    out_v,
    up_v,
    down_v,
    h_v,
    scaled_v,
    own_v,
    acc_v,
    branch_v,
    inv_v,
    send_v,
    recv_v,
    sq_send,
    sq_recv,
    cb_send,
    cb_recv,
    in_sem,
    out_sem,
    weight_sem,
    send_sem,
    recv_sem,
    sq_ssem,
    sq_rsem,
    cb_ssem,
    cb_rsem,
):
    k = lax.axis_index("ra")
    cb = lax.axis_index("cb")
    layers, hidden = up_v.shape[0], up_v.shape[2]
    splits, rows = h_v.shape[0], h_v.shape[1]
    chunk = send_v.shape[3]
    chunks = hidden // chunk
    jobs = splits * chunks
    early = jnp.where(2 * k < n, 0, 1)
    late = 1 - early
    early_hops = jnp.where(early == 0, k, n - 1 - k)
    has_early = early_hops > 0
    early_to = jnp.where(early == 0, k + 1, k - 1)
    late_to = jnp.where(early_hops > 0, jnp.where(late == 0, k + 1, k - 1), early_to)
    depth = jnp.maximum((n - 1 - 2 * early_hops) * LAG, 1)
    gap = max(0, chunks + (n - 1) * LAG + SLACK - jobs)

    def up_copy(layer):
        ref = (up_first, up_second)[layer]
        return pltpu.make_async_copy(ref, up_v.at[layer], weight_sem.at[layer])

    def down_copy(layer):
        ref = (down_first, down_second)[layer]
        return pltpu.make_async_copy(ref, down_v.at[layer], weight_sem.at[layers + layer])

    inputs = [pltpu.make_async_copy(tokens_ref, tokens_v, in_sem.at[0])]
    for i, ref in enumerate((gain_first, gain_second, gain_last)):
        inputs.append(pltpu.make_async_copy(ref, gain_v.at[i], in_sem.at[1 + i]))
    for copy in inputs:
        copy.start()
    up_copy(0).start()

    barrier = pltpu.get_barrier_semaphore()
    for off in range(1, n):
        pl.semaphore_signal(
            barrier, inc=1, device_id={"ra": lax.rem(k + off, n)}, device_id_type=MESH
        )
    for off in range(1, ncb):
        pl.semaphore_signal(
            barrier, inc=1, device_id={"cb": lax.rem(cb + off, ncb)}, device_id_type=MESH
        )
    for copy in inputs:
        copy.wait()
    for t in range(splits):
        h32 = tokens_v[t * rows : (t + 1) * rows, :].astype(F32)
        h_v[t] = h32
        scaled_v[0, t] = (h32 * gain_v[0]).astype(BF16)
    pl.semaphore_wait(barrier, n - 1 + ncb - 1)
    down_copy(0).start()
    up_copy(1).start()
    down_copy(1).start()

    def chain(direction, job, to):
        return pltpu.make_async_remote_copy(
            src_ref=send_v.at[direction, job],
            dst_ref=recv_v.at[direction, job],
            send_sem=send_sem.at[direction],
            recv_sem=recv_sem.at[direction, lax.rem(job, jobs)],
            device_id={"ra": to},
            device_id_type=MESH,
        )

    def sq_copy(level, t, source, to):
        return pltpu.make_async_remote_copy(
            src_ref=sq_send.at[level, t],
            dst_ref=sq_recv.at[level, t, source],
            send_sem=sq_ssem,
            recv_sem=sq_rsem.at[level, t],
            device_id={"ra": to},
            device_id_type=MESH,
        )

    def cb_copy(layer, t, source, to):
        return pltpu.make_async_remote_copy(
            src_ref=cb_send.at[layer, t],
            dst_ref=cb_recv.at[layer, t, source],
            send_sem=cb_ssem,
            recv_sem=cb_rsem.at[layer, t],
            device_id={"cb": to},
            device_id_type=MESH,
        )

    def of_all(ref, ssem, rsem, axis, to):
        return pltpu.make_async_remote_copy(
            src_ref=ref,
            dst_ref=ref,
            send_sem=ssem,
            recv_sem=rsem,
            device_id={axis: to},
            device_id_type=MESH,
        )

    diagonal = lax.broadcasted_iota(jnp.int32, (rows, 128), 0) == lax.broadcasted_iota(
        jnp.int32, (rows, 128), 1
    )

    def send_squares(level, t, h32):
        total = jnp.sum(h32 * h32, axis=1, keepdims=True)
        line = jnp.sum(jnp.where(diagonal, total, 0.0), axis=0, keepdims=True)
        sq_send[level, t] = line
        sq_recv[level, t, k] = line
        for off in range(1, n):
            sq_copy(level, t, k, lax.rem(k + off, n)).start()

    def inverse_of(level, t):
        peers = sq_recv.at[level, t, pl.ds(0, n - 1)]
        of_all(peers, sq_ssem, sq_rsem.at[level, t], "ra", lax.rem(k + 1, n)).wait_recv()
        total = sq_recv[level, t, 0]
        for source in range(1, n):
            total = total + sq_recv[level, t, source]
        line = lax.rsqrt(total * (1.0 / width) + EPS)
        column = jnp.sum(jnp.where(diagonal, line, 0.0), axis=1, keepdims=True)
        return jnp.broadcast_to(column, (rows, 128))

    def gather_branch(layer, t):
        peers = cb_recv.at[layer, t, pl.ds(0, ncb - 1)]
        of_all(peers, cb_ssem, cb_rsem.at[layer, t], "cb", lax.rem(cb + 1, ncb)).wait_recv()
        total = cb_recv[layer, t, 0].astype(F32)
        for source in range(1, ncb):
            total = total + cb_recv[layer, t, source].astype(F32)
        return (0.5 * h_v[t] + total).astype(BF16).astype(F32)

    for t in range(splits):
        send_squares(0, t, h_v[t])

    def multiply_up(level, t, c):
        columns = pl.ds(pl.multiple_of(c * chunk, chunk), chunk)
        own_v[(level * splits + t) * chunks + c] = jnp.dot(
            scaled_v[level, t], up_v[level, :, columns], preferred_element_type=F32
        )

    up_copy(0).wait()
    multiply_up(0, 0, 0)

    def step(s, _):
        s2 = s - depth
        level2 = jnp.where(s2 < jobs + gap, 0, 1)
        at2 = s2 - level2 * (jobs + gap)
        live2 = (s2 >= 0) & (at2 < jobs)
        at2 = jnp.where(live2, at2, 0)
        t2 = at2 // chunks
        c2 = at2 % chunks
        job2 = level2 * jobs + at2

        @pl.when(live2)
        def _():
            chain(late, job2, late_to).wait_recv()

            @pl.when(has_early)
            def _():
                send_v[late, job2] = (recv_v[late, job2].astype(F32) + own_v[job2]).astype(BF16)
                chain(late, job2, late_to).start()

        @pl.when(live2 & (c2 == 0))
        def _():
            inv_v[...] = inverse_of(level2, t2)

        for layer in range(layers):

            @pl.when(live2 & (job2 == layer * jobs))
            def _():
                down_copy(layer).wait()

        @pl.when(live2)
        def _():
            pre = (recv_v[late, job2].astype(F32) + acc_v[job2]) * inv_v[:, 0:1]
            hidden = jnp.square(jnp.maximum(pre, 0.0)).astype(BF16)
            rows_at = pl.ds(pl.multiple_of(c2 * chunk, chunk), chunk)
            part = jnp.dot(hidden, down_v[level2, rows_at, :], preferred_element_type=F32)

            @pl.when(c2 == 0)
            def _():
                branch_v[...] = part

            @pl.when(c2 > 0)
            def _():
                branch_v[...] += part

        @pl.when(live2 & (c2 == chunks - 1))
        def _():
            value = branch_v[...].astype(BF16)
            cb_send[level2, t2] = value
            cb_recv[level2, t2, cb] = value
            for off in range(1, ncb):
                cb_copy(level2, t2, cb, lax.rem(cb + off, ncb)).start()

        level = jnp.where(
            s < jobs + gap, 0, jnp.where(s < 2 * (jobs + gap), 1, 2)
        )
        at = s - level * (jobs + gap)
        live = at < jobs
        t = jnp.where(live, at // chunks, 0)
        c = at % chunks
        job = level * jobs + at

        @pl.when(live & (c == 0) & (level == 1))
        def _():
            h32 = gather_branch(0, t)
            h_v[t] = h32
            send_squares(1, t, h32)
            scaled_v[1, t] = (h32 * gain_v[1]).astype(BF16)

            @pl.when(at == 0)
            def _():
                up_copy(1).wait()

            multiply_up(1, t, 0)

        @pl.when(live & (c == 0) & (level == 2))
        def _():
            h32 = gather_branch(1, t)
            h_v[t] = h32
            send_squares(2, t, h32)

        @pl.when(live & (level < layers))
        def _():
            own = own_v[job]

            @pl.when(has_early)
            def _():
                chain(early, job, early_to).wait_recv()
                total = recv_v[early, job].astype(F32) + own
                send_v[early, job] = total.astype(BF16)
                acc_v[job] = total

            @pl.when(jnp.logical_not(has_early))
            def _():
                send_v[early, job] = own.astype(BF16)
                acc_v[job] = own

            chain(early, job, early_to).start()

        follows = (level < layers) & (at + 1 < jobs)
        near = jnp.where(follows, at + 1, 0)

        @pl.when(follows & ((level == 0) | (near % chunks > 0)))
        def _():
            multiply_up(level, near // chunks, near % chunks)

        return 0

    lax.fori_loop(0, 2 * (jobs + gap) + (splits - 1) * chunks + 1, step, 0)

    def out_copy():
        return pltpu.make_async_copy(out_v, out_ref, out_sem)

    for t in range(splits):
        inv = inverse_of(2, t)[:, 0:1]
        out_v[t * rows : (t + 1) * rows, :] = (h_v[t] * inv * gain_v[2]).astype(BF16)
    out_copy().start()

    of_all(send_v.at[early], send_sem.at[early], recv_sem.at[early, 0], "ra", early_to).wait_send()

    @pl.when(has_early)
    def _():
        of_all(send_v.at[late], send_sem.at[late], recv_sem.at[late, 0], "ra", late_to).wait_send()

    peers = sq_recv.at[:, :, pl.ds(0, n - 1)]
    of_all(peers, sq_ssem, sq_rsem.at[0, 0], "ra", lax.rem(k + 1, n)).wait_send()
    peers = cb_recv.at[:, :, pl.ds(0, ncb - 1)]
    of_all(peers, cb_ssem, cb_rsem.at[0, 0], "cb", lax.rem(cb + 1, ncb)).wait_send()
    out_copy().wait()


def local(n, ncb, *args):
    tokens, gain_first, up_first, down_first, gain_second, up_second, down_second, gain_last = args
    rows, cols = tokens.shape
    hidden = up_first.shape[1]
    chunk = min(CHUNK, hidden)
    chunks = hidden // chunk
    splits = SPLITS if rows % (16 * SPLITS) == 0 else 1
    part = rows // splits
    jobs = 2 * splits * chunks
    hbm = pl.BlockSpec(memory_space=pl.ANY)
    dma = pltpu.SemaphoreType.DMA
    return pl.pallas_call(
        functools.partial(kernel, n, ncb, cols * n),
        out_shape=jax.ShapeDtypeStruct((rows, cols), BF16),
        in_specs=[hbm] * 8,
        out_specs=hbm,
        scratch_shapes=[
            pltpu.VMEM((rows, cols), BF16),
            pltpu.VMEM((3, 1, cols), F32),
            pltpu.VMEM((rows, cols), BF16),
            pltpu.VMEM((2, cols, hidden), BF16),
            pltpu.VMEM((2, hidden, cols), BF16),
            pltpu.VMEM((splits, part, cols), F32),
            pltpu.VMEM((2, splits, part, cols), BF16),
            pltpu.VMEM((jobs, part, chunk), F32),
            pltpu.VMEM((jobs, part, chunk), F32),
            pltpu.VMEM((part, cols), F32),
            pltpu.VMEM((part, 128), F32),
            pltpu.VMEM((2, jobs, part, chunk), BF16),
            pltpu.VMEM((2, jobs, part, chunk), BF16),
            pltpu.VMEM((3, splits, 1, 128), F32),
            pltpu.VMEM((3, splits, n, 1, 128), F32),
            pltpu.VMEM((2, splits, part, cols), BF16),
            pltpu.VMEM((2, splits, ncb, part, cols), BF16),
            dma((4,)),
            dma,
            dma((4,)),
            dma((2,)),
            dma((2, jobs // 2)),
            dma,
            dma((3, splits)),
            dma,
            dma((2, splits)),
        ],
        compiler_params=pltpu.CompilerParams(
            collective_id=0, has_side_effects=True, vmem_limit_bytes=60 * 1024 * 1024
        ),
    )(
        tokens,
        gain_first.reshape(1, cols),
        up_first,
        down_first,
        gain_second.reshape(1, cols),
        up_second,
        down_second,
        gain_last.reshape(1, cols),
    )


def solution(mesh):
    return jax.shard_map(
        functools.partial(local, mesh.shape["ra"], mesh.shape["cb"]),
        mesh=mesh,
        in_specs=(
            P(("grp", "dp"), "ra"),
            P("ra"),
            P("ra", "cb"),
            P("cb", "ra"),
            P("ra"),
            P("ra", "cb"),
            P("cb", "ra"),
            P("ra"),
        ),
        out_specs=P(("grp", "dp"), "ra"),
        check_vma=False,
    )
```

profile of v0, /device:TPU:0, one launch (start us, length us, event | category | flops | bytes accessed | tf_op | source)
XLA Modules:
  0.0 50.5 jit_solution(2368067122721515758)
XLA Ops:
  0.0 49.1 %shard_map.82 = bf16[64,512]{1,0:T(8,128)(2,1)} custom-call(bf16[64,512]{1,0:T(8,128)(2,1)} %tokens_ref.1, f32[1,512]{1,0:T(1,128)} %bitcast.3, bf16[512,4096]{1,0:T(8,128)(2,1)} %up_first.1, bf16[4096,512]{1,0:T(8,128)(2,1)} %down_first.1, f32[1,512]{1,0:T(1,128)} %bitcast.4, bf16[512,4096]{1,0:T(8,128)(2,1)} %up_second.1, bf16[4096,512]{1,0:T(8,128)(2,1)} %down_second.1, ...), custom_call_target="tpu_custom_call" | custom-call | tf_op jit(solution)/shard_map/pallas_call | solution.py:334
  49.1 1.5 %copy.10 = bf16[64,512]{1,0:T(8,128)(2,1)} copy(bf16[64,512]{1,0:T(8,128)(2,1)} %shard_map.82) | data formatting | bytes 131072
where the time goes:
time: 50.7 us; the launch traced here: 50.5 us
  Pallas kernels  49.1 us (97%)
  local copies, waits for them, and re-layouts  1.47 us (3%)
    pallas_call x1, Pallas kernels, local(): pl.pallas_call(functools.partial(kernel, n, ncb, cols * n), out_shape=jax...  49.1 us
    unnamed x1, local copies, waits for them, and re-layouts  1.47 us

commit v1 on v0

v1 whole, which is shorter than its diff:
```python
import functools

import jax
import jax.numpy as jnp
from jax import lax
from jax.experimental import pallas as pl
from jax.experimental.pallas import tpu as pltpu
from jax.sharding import PartitionSpec as P

EPS = 1e-06
MESH = pl.DeviceIdType.MESH
F32, BF16 = jnp.float32, jnp.bfloat16

CHUNK = 1024
SPLITS = 4
PIECES = 2
LAG10 = 50
SLACK = 3


def kernel(
    n,
    ncb,
    width,
    tokens_ref,
    gain_first,
    up_first,
    down_first,
    gain_second,
    up_second,
    down_second,
    gain_last,
    out_ref,
    tokens_v,
    gain_v,
    out_v,
    up_v,
    down_v,
    h_v,
    scaled_v,
    own_v,
    acc_v,
    branch_v,
    inv_v,
    send_v,
    recv_v,
    sq_send,
    sq_recv,
    cb_send,
    cb_recv,
    in_sem,
    out_sem,
    up_sem,
    weight_sem,
    send_sem,
    recv_sem,
    sq_ssem,
    sq_rsem,
    cb_ssem,
    cb_rsem,
):
    k = lax.axis_index("ra")
    cb = lax.axis_index("cb")
    hidden = up_v.shape[2]
    splits, rows = h_v.shape[0], h_v.shape[1]
    chunk = own_v.shape[2]
    pieces = send_v.shape[2]
    piece = chunk // pieces
    chunks = hidden // chunk
    jobs = splits * chunks
    swap = ncb == 2 and splits >= 2
    early = jnp.where(2 * k < n, 0, 1)
    late = 1 - early
    early_hops = jnp.where(early == 0, k, n - 1 - k)
    has_early = early_hops > 0
    early_to = jnp.where(early == 0, k + 1, k - 1)
    late_to = jnp.where(early_hops > 0, jnp.where(late == 0, k + 1, k - 1), early_to)
    depth = jnp.maximum(((n - 1 - 2 * early_hops) * LAG10 + 9) // 10, 1)
    deepest = max(((n - 1) * LAG10 + 9) // 10, 1)
    gap = max(0, chunks + deepest + SLACK - jobs)
    if swap:
        gap = max(gap, deepest - (splits - 2) * chunks, deepest + SLACK - (splits - 1) * chunks)
    period = jobs + gap

    def up_copy(c):
        columns = pl.ds(c * chunk, chunk)
        return pltpu.make_async_copy(up_first.at[:, columns], up_v.at[0, :, columns], up_sem.at[c])

    def up_wait(c):
        columns = pl.ds(pl.multiple_of(c * chunk, chunk), chunk)
        pltpu.make_async_copy(
            up_first.at[:, columns], up_v.at[0, :, columns], up_sem.at[c]
        ).wait()

    up_next = pltpu.make_async_copy(up_second, up_v.at[1], weight_sem.at[2])

    def down_copy(layer):
        ref = (down_first, down_second)[layer]
        return pltpu.make_async_copy(ref, down_v.at[layer], weight_sem.at[layer])

    def split_of(level, slot):
        if not swap:
            return slot
        swapped = (lax.rem(cb + level, 2) == 0) & (slot >= splits - 2)
        return jnp.where(swapped, 2 * splits - 3 - slot, slot)

    inputs = [pltpu.make_async_copy(tokens_ref, tokens_v, in_sem.at[0])]
    for i, ref in enumerate((gain_first, gain_second, gain_last)):
        inputs.append(pltpu.make_async_copy(ref, gain_v.at[i], in_sem.at[1 + i]))
    for copy in inputs:
        copy.start()
    for c in range(chunks):
        up_copy(c).start()

    barrier = pltpu.get_barrier_semaphore()
    partners = [
        (i, j) for i in range(n) for j in range(ncb) if i + j > 0 and (swap or i * j == 0)
    ]
    for i, j in partners:
        pl.semaphore_signal(
            barrier,
            inc=1,
            device_id={"ra": lax.rem(k + i, n), "cb": lax.rem(cb + j, ncb)},
            device_id_type=MESH,
        )
    for copy in inputs:
        copy.wait()
    for t in range(splits):
        h32 = tokens_v[t * rows : (t + 1) * rows, :].astype(F32)
        h_v[t] = h32
        scaled_v[0, t] = (h32 * gain_v[0]).astype(BF16)

    def multiply_first(c):
        up_wait(c)
        columns = pl.ds(pl.multiple_of(c * chunk, chunk), chunk)
        every = jnp.concatenate([scaled_v[0, t] for t in range(splits)], axis=0)
        product = jnp.dot(every, up_v[0, :, columns], preferred_element_type=F32)
        for t in range(splits):
            own_v[t * chunks + c] = product[t * rows : (t + 1) * rows, :]

    multiply_first(0)
    pl.semaphore_wait(barrier, len(partners))
    down_copy(0).start()
    up_next.start()
    down_copy(1).start()

    def chain(direction, job, p, to):
        return pltpu.make_async_remote_copy(
            src_ref=send_v.at[direction, job, p],
            dst_ref=recv_v.at[direction, job, p],
            send_sem=send_sem.at[direction],
            recv_sem=recv_sem.at[direction, lax.rem(job, jobs), p],
            device_id={"ra": to},
            device_id_type=MESH,
        )

    def sq_copy(level, t, to, to_cb):
        return pltpu.make_async_remote_copy(
            src_ref=sq_send.at[level, t],
            dst_ref=sq_recv.at[level, t, k],
            send_sem=sq_ssem,
            recv_sem=sq_rsem.at[level, t],
            device_id={"ra": to, "cb": to_cb},
            device_id_type=MESH,
        )

    def cb_copy(layer, t, to):
        return pltpu.make_async_remote_copy(
            src_ref=cb_send.at[layer, t],
            dst_ref=cb_recv.at[layer, t, cb],
            send_sem=cb_ssem,
            recv_sem=cb_rsem.at[layer, t],
            device_id={"cb": to},
            device_id_type=MESH,
        )

    def of_all(ref, ssem, rsem, axis, to):
        return pltpu.make_async_remote_copy(
            src_ref=ref,
            dst_ref=ref,
            send_sem=ssem,
            recv_sem=rsem,
            device_id={axis: to},
            device_id_type=MESH,
        )

    diagonal = lax.broadcasted_iota(jnp.int32, (rows, 128), 0) == lax.broadcasted_iota(
        jnp.int32, (rows, 128), 1
    )

    def send_squares(level, t, h32, across=False):
        total = jnp.sum(h32 * h32, axis=1, keepdims=True)
        line = jnp.sum(jnp.where(diagonal, total, 0.0), axis=0, keepdims=True)
        sq_send[level, t] = line
        sq_recv[level, t, k] = line
        for off in range(1, n):
            sq_copy(level, t, lax.rem(k + off, n), cb).start()
        if across:
            for off in range(n):
                sq_copy(level, t, lax.rem(k + off, n), lax.rem(cb + 1, ncb)).start()

    def wait_squares(level, t, count):
        peers = sq_recv.at[level, t, pl.ds(0, count)]
        of_all(peers, sq_ssem, sq_rsem.at[level, t], "ra", lax.rem(k + 1, n)).wait_recv()

    def inverse_of(level, t):
        total = sq_recv[level, t, 0]
        for source in range(1, n):
            total = total + sq_recv[level, t, source]
        line = lax.rsqrt(total * (1.0 / width) + EPS)
        column = jnp.sum(jnp.where(diagonal, line, 0.0), axis=1, keepdims=True)
        return jnp.broadcast_to(column, (rows, 128))

    def gather_branch(layer, t):
        peers = cb_recv.at[layer, t, pl.ds(0, ncb - 1)]
        of_all(peers, cb_ssem, cb_rsem.at[layer, t], "cb", lax.rem(cb + 1, ncb)).wait_recv()
        total = cb_recv[layer, t, 0].astype(F32)
        for source in range(1, ncb):
            total = total + cb_recv[layer, t, source].astype(F32)
        return (0.5 * h_v[t] + total).astype(BF16).astype(F32)

    def multiply_up(t, c):
        columns = pl.ds(pl.multiple_of(c * chunk, chunk), chunk)
        own_v[(splits + t) * chunks + c] = jnp.dot(
            scaled_v[1, t], up_v[1, :, columns], preferred_element_type=F32
        )

    def multiply_down(level, job, c):
        total = None
        for p in range(pieces):
            at = slice(p * piece, (p + 1) * piece)
            pre = (recv_v[late, job, p].astype(F32) + acc_v[job, :, at]) * inv_v[:, 0:1]
            act = jnp.square(jnp.maximum(pre, 0.0)).astype(BF16)
            rows_at = pl.ds(pl.multiple_of(c * chunk + p * piece, piece), piece)
            part = jnp.dot(act, down_v[level, rows_at, :], preferred_element_type=F32)
            total = part if total is None else total + part
        branch_v[...] = jnp.where(c == 0, 0.0, branch_v[...]) + total

    branch_v[...] = jnp.zeros_like(branch_v)

    def place(s):
        level = jnp.where(s < period, 0, jnp.where(s < 2 * period, 1, 2))
        at = s - level * period
        live = at < jobs
        slot = jnp.where(live, at // chunks, 0)
        return level, at, live, slot, at % chunks

    finals = [j for j in range(splits - 2 if swap else splits)]
    steps = 2 * jobs + gap + deepest
    inside = [j for j in finals if 2 * period + j * chunks < steps]

    def step(s, _):
        s2 = s - depth
        level2 = jnp.where(s2 < period, 0, 1)
        at2 = s2 - level2 * period
        live2 = (s2 >= 0) & (at2 < jobs)
        at2 = jnp.where(live2, at2, 0)
        t2 = split_of(level2, at2 // chunks)
        c2 = at2 % chunks
        job2 = level2 * jobs + at2

        level, at, live, slot, c = place(s)
        t = split_of(level, slot)
        job = level * jobs + at
        own_at = (level * splits + t) * chunks + c
        sending = live & (level < 2)

        own_at2 = (level2 * splits + t2) * chunks + c2
        for p in range(pieces):
            part = slice(p * piece, (p + 1) * piece)

            @pl.when(live2)
            def _():
                chain(late, job2, p, late_to).wait_recv()

                @pl.when(has_early)
                def _():
                    total = recv_v[late, job2, p].astype(F32) + own_v[own_at2, :, part]
                    send_v[late, job2, p] = total.astype(BF16)
                    chain(late, job2, p, late_to).start()

            @pl.when(sending)
            def _():
                own = own_v[own_at, :, part]

                @pl.when(has_early)
                def _():
                    chain(early, job, p, early_to).wait_recv()
                    total = recv_v[early, job, p].astype(F32) + own
                    send_v[early, job, p] = total.astype(BF16)
                    acc_v[job, :, part] = total

                @pl.when(jnp.logical_not(has_early))
                def _():
                    send_v[early, job, p] = own.astype(BF16)
                    acc_v[job, :, part] = own

                chain(early, job, p, early_to).start()

        @pl.when(s == 0)
        def _():
            for i in range(splits):
                send_squares(0, i, h_v[i])

        @pl.when(sending & (level == 1) & (c == 0))
        def _():
            send_squares(1, t, h_v[t])

        @pl.when(live2 & (c2 == 0))
        def _():
            wait_squares(level2, t2, n - 1)
            inv_v[...] = inverse_of(level2, t2)

        for layer in range(2):

            @pl.when(live2 & (job2 == layer * jobs))
            def _():
                down_copy(layer).wait()

        level3, at3, live3, slot3, c3 = place(s + 1)
        t3 = split_of(level3, slot3)
        ahead = live3 & (level3 == 1)
        both = live2 & ahead & (c3 > 0)

        @pl.when(both)
        def _():
            multiply_up(t3, c3)
            multiply_down(level2, job2, c2)

        @pl.when(live2 & jnp.logical_not(both))
        def _():
            multiply_down(level2, job2, c2)

        @pl.when(live2 & (c2 == chunks - 1))
        def _():
            value = branch_v[...].astype(BF16)
            cb_send[level2, t2] = value
            cb_recv[level2, t2, cb] = value
            for off in range(1, ncb):
                cb_copy(level2, t2, lax.rem(cb + off, ncb)).start()

        @pl.when(ahead & (c3 == 0))
        def _():
            h32 = gather_branch(0, t3)
            h_v[t3] = h32
            scaled_v[1, t3] = (h32 * gain_v[1]).astype(BF16)

            @pl.when(at3 == 0)
            def _():
                up_next.wait()

        @pl.when(ahead & jnp.logical_not(both))
        def _():
            multiply_up(t3, c3)

        @pl.when(live3 & (level3 == 0) & (at3 < chunks))
        def _():
            multiply_first(c3)

        for j in inside:

            @pl.when(s == 2 * period + j * chunks)
            def _():
                h32 = gather_branch(1, j)
                h_v[j] = h32
                send_squares(2, j, h32)

        return 0

    lax.fori_loop(0, steps, step, 0)

    def out_copy(t):
        at = pl.ds(pl.multiple_of(t * rows, rows), rows)
        return pltpu.make_async_copy(out_v.at[at, :], out_ref.at[at, :], out_sem)

    def finish(t):
        inv = inverse_of(2, t)[:, 0:1]
        at = pl.ds(pl.multiple_of(t * rows, rows), rows)
        out_v[at, :] = (h_v[t] * inv * gain_v[2]).astype(BF16)
        out_copy(t).start()

    if swap:
        mine = split_of(1, splits - 1)
        other = split_of(1, splits - 2)
        h32 = gather_branch(1, mine)
        h_v[mine] = h32
        send_squares(2, mine, h32, across=True)
    for j in finals:
        if j not in inside:
            h32 = gather_branch(1, j)
            h_v[j] = h32
            send_squares(2, j, h32)
    for j in finals:
        wait_squares(2, j, n - 1)
        finish(j)
    if swap:
        h_v[other] = gather_branch(1, other)
        wait_squares(2, other, n)
        finish(other)
        wait_squares(2, mine, n - 1)
        finish(mine)

    of_all(send_v.at[early], send_sem.at[early], recv_sem.at[early, 0, 0], "ra", early_to).wait_send()

    @pl.when(has_early)
    def _():
        of_all(send_v.at[late], send_sem.at[late], recv_sem.at[late, 0, 0], "ra", late_to).wait_send()

    peers = sq_recv.at[:, :, pl.ds(0, n - 1)]
    of_all(peers, sq_ssem, sq_rsem.at[0, 0], "ra", lax.rem(k + 1, n)).wait_send()
    if swap:
        one = sq_recv.at[0, 0, pl.ds(0, 1)]
        of_all(one, sq_ssem, sq_rsem.at[0, 0], "ra", lax.rem(k + 1, n)).wait_send()
    peers = cb_recv.at[:, :, pl.ds(0, ncb - 1)]
    of_all(peers, cb_ssem, cb_rsem.at[0, 0], "cb", lax.rem(cb + 1, ncb)).wait_send()
    pltpu.make_async_copy(out_v, out_ref, out_sem).wait()


def local(n, ncb, *args):
    tokens, gain_first, up_first, down_first, gain_second, up_second, down_second, gain_last = args
    rows, cols = tokens.shape
    hidden = up_first.shape[1]
    chunk = min(CHUNK, hidden)
    chunks = hidden // chunk
    splits = SPLITS if rows % (16 * SPLITS) == 0 else 1
    part = rows // splits
    jobs = splits * chunks
    piece = chunk // PIECES
    hbm = pl.BlockSpec(memory_space=pl.ANY)
    dma = pltpu.SemaphoreType.DMA
    return pl.pallas_call(
        functools.partial(kernel, n, ncb, cols * n),
        out_shape=jax.ShapeDtypeStruct((rows, cols), BF16),
        in_specs=[hbm] * 8,
        out_specs=hbm,
        scratch_shapes=[
            pltpu.VMEM((rows, cols), BF16),
            pltpu.VMEM((3, 1, cols), F32),
            pltpu.VMEM((rows, cols), BF16),
            pltpu.VMEM((2, cols, hidden), BF16),
            pltpu.VMEM((2, hidden, cols), BF16),
            pltpu.VMEM((splits, part, cols), F32),
            pltpu.VMEM((2, splits, part, cols), BF16),
            pltpu.VMEM((2 * jobs, part, chunk), F32),
            pltpu.VMEM((2 * jobs, part, chunk), F32),
            pltpu.VMEM((part, cols), F32),
            pltpu.VMEM((part, 128), F32),
            pltpu.VMEM((2, 2 * jobs, PIECES, part, piece), BF16),
            pltpu.VMEM((2, 2 * jobs, PIECES, part, piece), BF16),
            pltpu.VMEM((3, splits, 1, 128), F32),
            pltpu.VMEM((3, splits, n, 1, 128), F32),
            pltpu.VMEM((2, splits, part, cols), BF16),
            pltpu.VMEM((2, splits, ncb, part, cols), BF16),
            dma((4,)),
            dma,
            dma((chunks,)),
            dma((3,)),
            dma((2,)),
            dma((2, jobs, PIECES)),
            dma,
            dma((3, splits)),
            dma,
            dma((2, splits)),
        ],
        compiler_params=pltpu.CompilerParams(
            collective_id=0, has_side_effects=True, vmem_limit_bytes=60 * 1024 * 1024
        ),
    )(
        tokens,
        gain_first.reshape(1, cols),
        up_first,
        down_first,
        gain_second.reshape(1, cols),
        up_second,
        down_second,
        gain_last.reshape(1, cols),
    )


def solution(mesh):
    return jax.shard_map(
        functools.partial(local, mesh.shape["ra"], mesh.shape["cb"]),
        mesh=mesh,
        in_specs=(
            P(("grp", "dp"), "ra"),
            P("ra"),
            P("ra", "cb"),
            P("cb", "ra"),
            P("ra"),
            P("ra", "cb"),
            P("cb", "ra"),
            P("ra"),
        ),
        out_specs=P(("grp", "dp"), "ra"),
        check_vma=False,
    )
```

time: 50.7 us -> 48.6 us (0.959)
  Pallas kernels: 49.1 us -> 46.9 us
    pallas_call x1, Pallas kernels: 49.1 us -> 46.9 us  [local(): pl.pallas_call(functools.partial(kernel, n, ncb, cols * n), out_shape=jax...]
where the time goes in v1:
time: 48.6 us; the launch traced here: 48.4 us
  Pallas kernels  46.9 us (97%)
  local copies, waits for them, and re-layouts  1.47 us (3%)
    pallas_call x1, Pallas kernels, local(): pl.pallas_call(functools.partial(kernel, n, ncb, cols * n), out_shape=jax...  46.9 us
    unnamed x1, local copies, waits for them, and re-layouts  1.47 us

profile of v1, /device:TPU:0, one launch (start us, length us, event | category | flops | bytes accessed | tf_op | source)
XLA Modules:
  0.0 48.4 jit_solution(13732323020591236684)
XLA Ops:
  0.0 46.9 %shard_map.82 = bf16[64,512]{1,0:T(8,128)(2,1)} custom-call(bf16[64,512]{1,0:T(8,128)(2,1)} %tokens_ref.1, f32[1,512]{1,0:T(1,128)} %bitcast.3, bf16[512,4096]{1,0:T(8,128)(2,1)} %up_first.1, bf16[4096,512]{1,0:T(8,128)(2,1)} %down_first.1, f32[1,512]{1,0:T(1,128)} %bitcast.4, bf16[512,4096]{1,0:T(8,128)(2,1)} %up_second.1, bf16[4096,512]{1,0:T(8,128)(2,1)} %down_second.1, ...), custom_call_target="tpu_custom_call" | custom-call | tf_op jit(solution)/shard_map/pallas_call | solution.py:431
  46.9 1.5 %copy.10 = bf16[64,512]{1,0:T(8,128)(2,1)} copy(bf16[64,512]{1,0:T(8,128)(2,1)} %shard_map.82) | data formatting | bytes 131072

commit v2 on v1

--- a/solution.py
+++ b/solution.py
@@ -14,29 +14,31 @@
 CHUNK = 1024
 SPLITS = 4
 PIECES = 2
-LAG10 = 50
-SLACK = 3
+LAG10 = (45, 40)
+SLACK = (3, 3)
+LIMIT = 55100
 
 
 def kernel(
     n,
     ncb,
+    moved,
     width,
     tokens_ref,
-    gain_first,
+    gains,
     up_first,
     down_first,
-    gain_second,
     up_second,
     down_second,
-    gain_last,
     out_ref,
     tokens_v,
-    gain_v,
-    out_v,
+    extra_v,
+    done_v,
+    back_v,
     up_v,
     down_v,
     h_v,
+    entry_v,
     scaled_v,
     own_v,
     acc_v,
@@ -49,7 +51,7 @@
     cb_send,
     cb_recv,
     in_sem,
-    out_sem,
+    pass_sem,
     up_sem,
     weight_sem,
     send_sem,
@@ -60,26 +62,33 @@
     cb_rsem,
 ):
     k = lax.axis_index("ra")
+    second = lax.axis_index("dp") > 0
+    other_core = 1 - lax.axis_index("dp")
     cb = lax.axis_index("cb")
     hidden = up_v.shape[2]
-    splits, rows = h_v.shape[0], h_v.shape[1]
+    most, rows = h_v.shape[0], h_v.shape[1]
     chunk = own_v.shape[2]
     pieces = send_v.shape[2]
     piece = chunk // pieces
     chunks = hidden // chunk
+    most_jobs = most * chunks
+    swap = ncb == 2 and most - 2 * moved >= 2
+    splits = jnp.where(second, most, most - 2 * moved)
     jobs = splits * chunks
-    swap = ncb == 2 and splits >= 2
     early = jnp.where(2 * k < n, 0, 1)
     late = 1 - early
     early_hops = jnp.where(early == 0, k, n - 1 - k)
     has_early = early_hops > 0
     early_to = jnp.where(early == 0, k + 1, k - 1)
     late_to = jnp.where(early_hops > 0, jnp.where(late == 0, k + 1, k - 1), early_to)
-    depth = jnp.maximum(((n - 1 - 2 * early_hops) * LAG10 + 9) // 10, 1)
-    deepest = max(((n - 1) * LAG10 + 9) // 10, 1)
-    gap = max(0, chunks + deepest + SLACK - jobs)
+    lags = jnp.where(second, LAG10[1], LAG10[0])
+    slack = jnp.where(second, SLACK[1], SLACK[0])
+    depth = jnp.maximum(((n - 1 - 2 * early_hops) * lags + 9) // 10, 1)
+    deepest = jnp.maximum(((n - 1) * lags + 9) // 10, 1)
+    gap = jnp.maximum(chunks + deepest + slack - jobs, 0)
     if swap:
-        gap = max(gap, deepest - (splits - 2) * chunks, deepest + SLACK - (splits - 1) * chunks)
+        gap = jnp.maximum(gap, deepest - (splits - 2) * chunks)
+        gap = jnp.maximum(gap, deepest + slack - (splits - 1) * chunks)
     period = jobs + gap
 
     def up_copy(c):
@@ -104,13 +113,9 @@
         swapped = (lax.rem(cb + level, 2) == 0) & (slot >= splits - 2)
         return jnp.where(swapped, 2 * splits - 3 - slot, slot)
 
-    inputs = [pltpu.make_async_copy(tokens_ref, tokens_v, in_sem.at[0])]
-    for i, ref in enumerate((gain_first, gain_second, gain_last)):
-        inputs.append(pltpu.make_async_copy(ref, gain_v.at[i], in_sem.at[1 + i]))
-    for copy in inputs:
-        copy.start()
-    for c in range(chunks):
-        up_copy(c).start()
+    tokens_in = pltpu.make_async_copy(tokens_ref, tokens_v, in_sem)
+    tokens_in.start()
+    up_copy(0).start()
 
     barrier = pltpu.get_barrier_semaphore()
     partners = [
@@ -123,23 +128,64 @@
             device_id={"ra": lax.rem(k + i, n), "cb": lax.rem(cb + j, ncb)},
             device_id_type=MESH,
         )
-    for copy in inputs:
-        copy.wait()
-    for t in range(splits):
-        h32 = tokens_v[t * rows : (t + 1) * rows, :].astype(F32)
-        h_v[t] = h32
-        scaled_v[0, t] = (h32 * gain_v[0]).astype(BF16)
-
+    if moved:
+        pl.semaphore_signal(
+            barrier, inc=1, device_id={"dp": other_core}, device_id_type=MESH
+        )
+
+    def to_core(src, dst, i):
+        return pltpu.make_async_remote_copy(
+            src_ref=src,
+            dst_ref=dst,
+            send_sem=pass_sem.at[2 * i],
+            recv_sem=pass_sem.at[2 * i + 1],
+            device_id={"dp": other_core},
+            device_id_type=MESH,
+        )
+
+    last = most - 1 - moved
+    lent = to_core(tokens_v.at[pl.ds(last * rows, rows), :], extra_v, 0)
+    given = to_core(done_v, back_v, 1)
+
+    def tile_of(i):
+        return i + jnp.where(second, moved, 0) if i > 1 else i
+
+    tokens_in.wait()
+    for c in range(1, chunks):
+        up_copy(c).start()
     def multiply_first(c):
         up_wait(c)
         columns = pl.ds(pl.multiple_of(c * chunk, chunk), chunk)
-        every = jnp.concatenate([scaled_v[0, t] for t in range(splits)], axis=0)
-        product = jnp.dot(every, up_v[0, :, columns], preferred_element_type=F32)
-        for t in range(splits):
-            own_v[t * chunks + c] = product[t * rows : (t + 1) * rows, :]
-
+        product = jnp.dot(entry_v[...], up_v[0, :, columns], preferred_element_type=F32)
+        for i in range(most - moved):
+            own_v[tile_of(i) * chunks + c] = product[i * rows : (i + 1) * rows, :]
+
+    def multiply_extra():
+        for c in range(chunks):
+            columns = pl.ds(c * chunk, chunk)
+            own_v[2 * chunks + c] = jnp.dot(
+                scaled_v[0], up_v[0, :, columns], preferred_element_type=F32
+            )
+
+    ready = has_early
+    for i in range(most - moved):
+        tile = tokens_v[i * rows : (i + 1) * rows, :].astype(F32)
+        h_v[tile_of(i)] = tile
+        entry_v[i * rows : (i + 1) * rows, :] = (tile * gains[0:1, :]).astype(BF16)
     multiply_first(0)
-    pl.semaphore_wait(barrier, len(partners))
+
+    @pl.when(ready)
+    def _():
+        for c in range(1, chunks):
+            multiply_first(c)
+
+    pl.semaphore_wait(barrier, len(partners) + moved)
+    if moved:
+
+        @pl.when(jnp.logical_not(second))
+        def _():
+            lent.start()
+
     down_copy(0).start()
     up_next.start()
     down_copy(1).start()
@@ -149,7 +195,7 @@
             src_ref=send_v.at[direction, job, p],
             dst_ref=recv_v.at[direction, job, p],
             send_sem=send_sem.at[direction],
-            recv_sem=recv_sem.at[direction, lax.rem(job, jobs), p],
+            recv_sem=recv_sem.at[direction, lax.rem(job, most_jobs), p],
             device_id={"ra": to},
             device_id_type=MESH,
         )
@@ -221,8 +267,8 @@
 
     def multiply_up(t, c):
         columns = pl.ds(pl.multiple_of(c * chunk, chunk), chunk)
-        own_v[(splits + t) * chunks + c] = jnp.dot(
-            scaled_v[1, t], up_v[1, :, columns], preferred_element_type=F32
+        own_v[(most + t) * chunks + c] = jnp.dot(
+            scaled_v[1 + t], up_v[1, :, columns], preferred_element_type=F32
         )
 
     def multiply_down(level, job, c):
@@ -245,9 +291,13 @@
         slot = jnp.where(live, at // chunks, 0)
         return level, at, live, slot, at % chunks
 
-    finals = [j for j in range(splits - 2 if swap else splits)]
     steps = 2 * jobs + gap + deepest
-    inside = [j for j in finals if 2 * period + j * chunks < steps]
+    plain = splits - 2 if swap else splits
+
+    def close(j):
+        h32 = gather_branch(1, j)
+        h_v[j] = h32
+        send_squares(2, j, h32)
 
     def step(s, _):
         s2 = s - depth
@@ -257,15 +307,15 @@
         at2 = jnp.where(live2, at2, 0)
         t2 = split_of(level2, at2 // chunks)
         c2 = at2 % chunks
-        job2 = level2 * jobs + at2
+        job2 = level2 * most_jobs + at2
 
         level, at, live, slot, c = place(s)
         t = split_of(level, slot)
-        job = level * jobs + at
-        own_at = (level * splits + t) * chunks + c
+        job = level * most_jobs + at
+        own_at = (level * most + t) * chunks + c
         sending = live & (level < 2)
 
-        own_at2 = (level2 * splits + t2) * chunks + c2
+        own_at2 = (level2 * most + t2) * chunks + c2
         for p in range(pieces):
             part = slice(p * piece, (p + 1) * piece)
 
@@ -299,8 +349,22 @@
 
         @pl.when(s == 0)
         def _():
-            for i in range(splits):
-                send_squares(0, i, h_v[i])
+            for i in range(most):
+
+                @pl.when((i < splits) & jnp.logical_not(second & (i == 2 * moved) & (moved > 0)))
+                def _():
+                    send_squares(0, i, h_v[i])
+
+        if moved:
+
+            @pl.when(second & (s == chunks - 1))
+            def _():
+                lent.wait_recv()
+                h32 = extra_v[...].astype(F32)
+                h_v[2] = h32
+                scaled_v[0] = (h32 * gains[0:1, :]).astype(BF16)
+                multiply_extra()
+                send_squares(0, 2, h32)
 
         @pl.when(sending & (level == 1) & (c == 0))
         def _():
@@ -313,7 +377,7 @@
 
         for layer in range(2):
 
-            @pl.when(live2 & (job2 == layer * jobs))
+            @pl.when(live2 & (job2 == layer * most_jobs))
             def _():
                 down_copy(layer).wait()
 
@@ -343,7 +407,7 @@
         def _():
             h32 = gather_branch(0, t3)
             h_v[t3] = h32
-            scaled_v[1, t3] = (h32 * gain_v[1]).astype(BF16)
+            scaled_v[1 + t3] = (h32 * gains[1:1 + 1, :]).astype(BF16)
 
             @pl.when(at3 == 0)
             def _():
@@ -353,31 +417,27 @@
         def _():
             multiply_up(t3, c3)
 
-        @pl.when(live3 & (level3 == 0) & (at3 < chunks))
+        @pl.when(live3 & (level3 == 0) & (at3 < chunks) & jnp.logical_not(ready))
         def _():
             multiply_first(c3)
 
-        for j in inside:
-
-            @pl.when(s == 2 * period + j * chunks)
+        for j in range(most):
+
+            @pl.when((j < plain) & (s == 2 * period + j * chunks))
             def _():
-                h32 = gather_branch(1, j)
-                h_v[j] = h32
-                send_squares(2, j, h32)
+                close(j)
 
         return 0
 
     lax.fori_loop(0, steps, step, 0)
 
-    def out_copy(t):
-        at = pl.ds(pl.multiple_of(t * rows, rows), rows)
-        return pltpu.make_async_copy(out_v.at[at, :], out_ref.at[at, :], out_sem)
+    def normed(t):
+        inv = inverse_of(2, t)[:, 0:1]
+        return (h_v[t] * inv * gains[2:3, :]).astype(BF16)
 
     def finish(t):
-        inv = inverse_of(2, t)[:, 0:1]
-        at = pl.ds(pl.multiple_of(t * rows, rows), rows)
-        out_v[at, :] = (h_v[t] * inv * gain_v[2]).astype(BF16)
-        out_copy(t).start()
+        row = t - jnp.where(second & (t > 2), moved, 0)
+        out_ref[pl.ds(pl.multiple_of(row * rows, rows), rows), :] = normed(t)
 
     if swap:
         mine = split_of(1, splits - 1)
@@ -385,14 +445,32 @@
         h32 = gather_branch(1, mine)
         h_v[mine] = h32
         send_squares(2, mine, h32, across=True)
-    for j in finals:
-        if j not in inside:
-            h32 = gather_branch(1, j)
-            h_v[j] = h32
-            send_squares(2, j, h32)
-    for j in finals:
-        wait_squares(2, j, n - 1)
-        finish(j)
+    for j in range(most):
+
+        @pl.when((j < plain) & (2 * period + j * chunks >= steps))
+        def _():
+            close(j)
+
+    order = [2, 0, 1] + list(range(3, most)) if moved else list(range(most))
+    for j in order:
+
+        @pl.when(j < plain)
+        def _():
+            wait_squares(2, j, n - 1)
+            if moved and j == 2:
+
+                @pl.when(second)
+                def _():
+                    done_v[...] = normed(2)
+                    given.start()
+
+                @pl.when(jnp.logical_not(second))
+                def _():
+                    finish(2)
+
+            else:
+                finish(j)
+
     if swap:
         h_v[other] = gather_branch(1, other)
         wait_squares(2, other, n)
@@ -400,23 +478,53 @@
         wait_squares(2, mine, n - 1)
         finish(mine)
 
-    of_all(send_v.at[early], send_sem.at[early], recv_sem.at[early, 0, 0], "ra", early_to).wait_send()
-
-    @pl.when(has_early)
-    def _():
-        of_all(send_v.at[late], send_sem.at[late], recv_sem.at[late, 0, 0], "ra", late_to).wait_send()
-
-    peers = sq_recv.at[:, :, pl.ds(0, n - 1)]
-    of_all(peers, sq_ssem, sq_rsem.at[0, 0], "ra", lax.rem(k + 1, n)).wait_send()
-    if swap:
-        one = sq_recv.at[0, 0, pl.ds(0, 1)]
-        of_all(one, sq_ssem, sq_rsem.at[0, 0], "ra", lax.rem(k + 1, n)).wait_send()
-    peers = cb_recv.at[:, :, pl.ds(0, ncb - 1)]
-    of_all(peers, cb_ssem, cb_rsem.at[0, 0], "cb", lax.rem(cb + 1, ncb)).wait_send()
-    pltpu.make_async_copy(out_v, out_ref, out_sem).wait()
-
-
-def local(n, ncb, *args):
+    def wait_sends(count):
+        sent = 2 * count * chunks
+        of_all(
+            send_v.at[early, pl.ds(0, sent)],
+            send_sem.at[early],
+            recv_sem.at[early, 0, 0],
+            "ra",
+            early_to,
+        ).wait_send()
+
+        @pl.when(has_early)
+        def _():
+            of_all(
+                send_v.at[late, pl.ds(0, sent)],
+                send_sem.at[late],
+                recv_sem.at[late, 0, 0],
+                "ra",
+                late_to,
+            ).wait_send()
+
+        peers = sq_recv.at[:, pl.ds(0, count), pl.ds(0, n - 1)]
+        of_all(peers, sq_ssem, sq_rsem.at[0, 0], "ra", lax.rem(k + 1, n)).wait_send()
+        if swap:
+            one = sq_recv.at[0, 0, pl.ds(0, 1)]
+            of_all(one, sq_ssem, sq_rsem.at[0, 0], "ra", lax.rem(k + 1, n)).wait_send()
+        peers = cb_recv.at[:, pl.ds(0, count), pl.ds(0, ncb - 1)]
+        of_all(peers, cb_ssem, cb_rsem.at[0, 0], "cb", lax.rem(cb + 1, ncb)).wait_send()
+
+    if moved:
+
+        @pl.when(second)
+        def _():
+            wait_sends(most)
+            given.wait_send()
+
+        @pl.when(jnp.logical_not(second))
+        def _():
+            wait_sends(most - 2)
+            lent.wait_send()
+            given.wait_recv()
+            out_ref[last * rows : (last + 1) * rows, :] = back_v[...]
+
+    else:
+        wait_sends(most)
+
+
+def local(n, ncb, ndp, *args):
     tokens, gain_first, up_first, down_first, gain_second, up_second, down_second, gain_last = args
     rows, cols = tokens.shape
     hidden = up_first.shape[1]
@@ -424,62 +532,65 @@
     chunks = hidden // chunk
     splits = SPLITS if rows % (16 * SPLITS) == 0 else 1
     part = rows // splits
-    jobs = splits * chunks
+    moved = int(ndp == 2 and splits >= 4)
+    most = splits + moved
+    jobs = most * chunks
     piece = chunk // PIECES
     hbm = pl.BlockSpec(memory_space=pl.ANY)
+    vm = pl.BlockSpec(memory_space=pltpu.VMEM)
     dma = pltpu.SemaphoreType.DMA
     return pl.pallas_call(
-        functools.partial(kernel, n, ncb, cols * n),
+        functools.partial(kernel, n, ncb, moved, cols * n),
         out_shape=jax.ShapeDtypeStruct((rows, cols), BF16),
-        in_specs=[hbm] * 8,
-        out_specs=hbm,
+        in_specs=[hbm, vm] + [hbm] * 4,
+        out_specs=vm,
         scratch_shapes=[
             pltpu.VMEM((rows, cols), BF16),
-            pltpu.VMEM((3, 1, cols), F32),
-            pltpu.VMEM((rows, cols), BF16),
+            pltpu.VMEM((part, cols), BF16),
+            pltpu.VMEM((part, cols), BF16),
+            pltpu.VMEM((part, cols), BF16),
             pltpu.VMEM((2, cols, hidden), BF16),
             pltpu.VMEM((2, hidden, cols), BF16),
-            pltpu.VMEM((splits, part, cols), F32),
-            pltpu.VMEM((2, splits, part, cols), BF16),
+            pltpu.VMEM((most, part, cols), F32),
+            pltpu.VMEM((rows, cols), BF16),
+            pltpu.VMEM((1 + most, part, cols), BF16),
             pltpu.VMEM((2 * jobs, part, chunk), F32),
             pltpu.VMEM((2 * jobs, part, chunk), F32),
             pltpu.VMEM((part, cols), F32),
             pltpu.VMEM((part, 128), F32),
             pltpu.VMEM((2, 2 * jobs, PIECES, part, piece), BF16),
             pltpu.VMEM((2, 2 * jobs, PIECES, part, piece), BF16),
-            pltpu.VMEM((3, splits, 1, 128), F32),
-            pltpu.VMEM((3, splits, n, 1, 128), F32),
-            pltpu.VMEM((2, splits, part, cols), BF16),
-            pltpu.VMEM((2, splits, ncb, part, cols), BF16),
+            pltpu.VMEM((3, most, 1, 128), F32),
+            pltpu.VMEM((3, most, n, 1, 128), F32),
+            pltpu.VMEM((2, most, part, cols), BF16),
+            pltpu.VMEM((2, most, ncb, part, cols), BF16),
+            dma,
             dma((4,)),
-            dma,
             dma((chunks,)),
             dma((3,)),
             dma((2,)),
             dma((2, jobs, PIECES)),
             dma,
-            dma((3, splits)),
+            dma((3, most)),
             dma,
-            dma((2, splits)),
+            dma((2, most)),
         ],
         compiler_params=pltpu.CompilerParams(
-            collective_id=0, has_side_effects=True, vmem_limit_bytes=60 * 1024 * 1024
+            collective_id=0, has_side_effects=True, vmem_limit_bytes=LIMIT * 1024
         ),
     )(
         tokens,
-        gain_first.reshape(1, cols),
+        jnp.stack([gain_first, gain_second, gain_last]),
         up_first,
         down_first,
-        gain_second.reshape(1, cols),
         up_second,
         down_second,
-        gain_last.reshape(1, cols),
     )
 
 
 def solution(mesh):
     return jax.shard_map(
-        functools.partial(local, mesh.shape["ra"], mesh.shape["cb"]),
+        functools.partial(local, mesh.shape["ra"], mesh.shape["cb"], mesh.shape["dp"]),
         mesh=mesh,
         in_specs=(
             P(("grp", "dp"), "ra"),

time: 48.6 us -> 45.5 us (0.936)
  Pallas kernels: 46.9 us -> 44 us
  local copies, waits for them, and re-layouts: 1.47 us -> 0.63 us
  other arithmetic: 0 us -> 0.72 us
    pallas_call x1, Pallas kernels: 46.9 us -> 44 us  [local(): pl.pallas_call(functools.partial(kernel, n, ncb, moved, cols * n), out_sh...]
    unnamed x1, local copies, waits for them, and re-layouts: 1.47 us -> 0.63 us
    another operation x0 -> x1, other arithmetic: none -> 0.72 us  [local(): jnp.stack([gain_first, gain_second, gain_last])]
where the time goes in v2:
time: 45.5 us; the launch traced here: 45.4 us
  Pallas kernels  44 us (97%)
  other arithmetic  0.72 us (2%)
  local copies, waits for them, and re-layouts  0.63 us (1%)
    pallas_call x1, Pallas kernels, local(): pl.pallas_call(functools.partial(kernel, n, ncb, moved, cols * n), out_sh...  44 us

profile of v2, /device:TPU:0, one launch (start us, length us, event | category | flops | bytes accessed | tf_op | source)
XLA Modules:
  0.0 45.4 jit_solution(4701959686762623970)
XLA Ops:
  0.0 0.7 %pad_maximum_fusion.gains = f32[3,512]{1,0:T(4,128)S(1)} fusion(f32[1,512]{1,0:T(1,128)} %bitcast.3, f32[1,512]{1,0:T(1,128)} %bitcast.4, f32[1,512]{1,0:T(1,128)} %bitcast.5), kind=kLoop, calls=%fused_computation | loop fusion | flops 3072 | bytes 12288 | tf_op jit(solution)/shard_map/stack | solution.py:583
  0.7 44.0 %shard_map.82 = bf16[64,512]{1,0:T(8,128)(2,1)S(1)} custom-call(bf16[64,512]{1,0:T(8,128)(2,1)} %tokens_ref.1, f32[3,512]{1,0:T(4,128)S(1)} %pad_maximum_fusion.gains, bf16[512,4096]{1,0:T(8,128)(2,1)} %up_first.1, bf16[4096,512]{1,0:T(8,128)(2,1)} %down_first.1, bf16[512,4096]{1,0:T(8,128)(2,1)} %up_second.1, bf16[4096,512]{1,0:T(8,128)(2,1)} %down_second.1), custom_call_target="tpu_custom_call" | custom-call | tf_op jit(solution)/shard_map/pallas_call | solution.py:542
  44.7 0.6 %copy.10 = bf16[64,512]{1,0:T(8,128)(2,1)} copy(bf16[64,512]{1,0:T(8,128)(2,1)S(1)} %shard_map.82) | data formatting | bytes 131072

commit v3 on v2

--- a/solution.py
+++ b/solution.py
@@ -14,8 +14,8 @@
 CHUNK = 1024
 SPLITS = 4
 PIECES = 2
-LAG10 = (45, 40)
-SLACK = (3, 3)
+LAG10 = (40, 40)
+SLACK = (2, 3)
 LIMIT = 55100
 
 
@@ -299,6 +299,17 @@
         h_v[j] = h32
         send_squares(2, j, h32)
 
+    def first_squares():
+        for i in range(most):
+
+            @pl.when((i < splits) & jnp.logical_not(second & (i == 2 * moved) & (moved > 0)))
+            def _():
+                send_squares(0, i, h_v[i])
+
+    @pl.when(has_early)
+    def _():
+        first_squares()
+
     def step(s, _):
         s2 = s - depth
         level2 = jnp.where(s2 < period, 0, 1)
@@ -347,13 +358,9 @@
 
                 chain(early, job, p, early_to).start()
 
-        @pl.when(s == 0)
-        def _():
-            for i in range(most):
-
-                @pl.when((i < splits) & jnp.logical_not(second & (i == 2 * moved) & (moved > 0)))
-                def _():
-                    send_squares(0, i, h_v[i])
+        @pl.when((s == 0) & jnp.logical_not(has_early))
+        def _():
+            first_squares()
 
         if moved:
 
@@ -366,7 +373,7 @@
                 multiply_extra()
                 send_squares(0, 2, h32)
 
-        @pl.when(sending & (level == 1) & (c == 0))
+        @pl.when(sending & (level == 1) & (c == 0) & jnp.logical_not(has_early))
         def _():
             send_squares(1, t, h_v[t])
 
@@ -416,6 +423,10 @@
         @pl.when(ahead & jnp.logical_not(both))
         def _():
             multiply_up(t3, c3)
+
+        @pl.when(ahead & (c3 == 0) & has_early)
+        def _():
+            send_squares(1, t3, h_v[t3])
 
         @pl.when(live3 & (level3 == 0) & (at3 < chunks) & jnp.logical_not(ready))
         def _():

time: 45.5 us -> 45.2 us (level)
  no operation moved by 1% of the time
where the time goes in v3:
time: 45.2 us; the launch traced here: 45 us
  Pallas kernels  43.6 us (96%)
  other arithmetic  0.72 us (2%)
  local copies, waits for them, and re-layouts  0.63 us (1%)
    pallas_call x1, Pallas kernels, local(): pl.pallas_call(functools.partial(kernel, n, ncb, moved, cols * n), out_sh...  43.6 us

profile of v3, /device:TPU:0, one launch (start us, length us, event | category | flops | bytes accessed | tf_op | source)
XLA Modules:
  0.0 45.0 jit_solution(10926333517466116679)
XLA Ops:
  0.0 0.7 %pad_maximum_fusion.gains = f32[3,512]{1,0:T(4,128)S(1)} fusion(f32[1,512]{1,0:T(1,128)} %bitcast.3, f32[1,512]{1,0:T(1,128)} %bitcast.4, f32[1,512]{1,0:T(1,128)} %bitcast.5), kind=kLoop, calls=%fused_computation | loop fusion | flops 3072 | bytes 12288 | tf_op jit(solution)/shard_map/stack | solution.py:594
  0.7 43.6 %shard_map.82 = bf16[64,512]{1,0:T(8,128)(2,1)S(1)} custom-call(bf16[64,512]{1,0:T(8,128)(2,1)} %tokens_ref.1, f32[3,512]{1,0:T(4,128)S(1)} %pad_maximum_fusion.gains, bf16[512,4096]{1,0:T(8,128)(2,1)} %up_first.1, bf16[4096,512]{1,0:T(8,128)(2,1)} %down_first.1, bf16[512,4096]{1,0:T(8,128)(2,1)} %up_second.1, bf16[4096,512]{1,0:T(8,128)(2,1)} %down_second.1), custom_call_target="tpu_custom_call" | custom-call | tf_op jit(solution)/shard_map/pallas_call | solution.py:553
  44.4 0.6 %copy.10 = bf16[64,512]{1,0:T(8,128)(2,1)} copy(bf16[64,512]{1,0:T(8,128)(2,1)S(1)} %shard_map.82) | data formatting | bytes 131072

commit v4 on v3

--- a/solution.py
+++ b/solution.py
@@ -14,6 +14,7 @@
 CHUNK = 1024
 SPLITS = 4
 PIECES = 2
+RING = 16
 LAG10 = (40, 40)
 SLACK = (2, 3)
 LIMIT = 55100
@@ -195,7 +196,7 @@
             src_ref=send_v.at[direction, job, p],
             dst_ref=recv_v.at[direction, job, p],
             send_sem=send_sem.at[direction],
-            recv_sem=recv_sem.at[direction, lax.rem(job, most_jobs), p],
+            recv_sem=recv_sem.at[direction, lax.rem(job, recv_sem.shape[1]), p],
             device_id={"ra": to},
             device_id_type=MESH,
         )
@@ -580,7 +581,7 @@
             dma((chunks,)),
             dma((3,)),
             dma((2,)),
-            dma((2, jobs, PIECES)),
+            dma((2, min(jobs, RING) if n == 4 else jobs, PIECES)),
             dma,
             dma((3, most)),
             dma,

time: 45.2 us -> 45.1 us (level)
  no operation moved by 1% of the time
where the time goes in v4:
time: 45.1 us; the launch traced here: 44.9 us
  Pallas kernels  43.6 us (97%)
  other arithmetic  0.72 us (2%)
  local copies, waits for them, and re-layouts  0.63 us (1%)
    pallas_call x1, Pallas kernels, local(): pl.pallas_call(functools.partial(kernel, n, ncb, moved, cols * n), out_sh...  43.6 us

profile of v4, /device:TPU:0, one launch (start us, length us, event | category | flops | bytes accessed | tf_op | source)
XLA Modules:
  0.0 44.9 jit_solution(7164747835940212941)
XLA Ops:
  0.0 0.7 %pad_maximum_fusion.gains = f32[3,512]{1,0:T(4,128)S(1)} fusion(f32[1,512]{1,0:T(1,128)} %bitcast.3, f32[1,512]{1,0:T(1,128)} %bitcast.4, f32[1,512]{1,0:T(1,128)} %bitcast.5), kind=kLoop, calls=%fused_computation | loop fusion | flops 3072 | bytes 12288 | tf_op jit(solution)/shard_map/stack | solution.py:595
  0.7 43.6 %shard_map.82 = bf16[64,512]{1,0:T(8,128)(2,1)S(1)} custom-call(bf16[64,512]{1,0:T(8,128)(2,1)} %tokens_ref.1, f32[3,512]{1,0:T(4,128)S(1)} %pad_maximum_fusion.gains, bf16[512,4096]{1,0:T(8,128)(2,1)} %up_first.1, bf16[4096,512]{1,0:T(8,128)(2,1)} %down_first.1, bf16[512,4096]{1,0:T(8,128)(2,1)} %up_second.1, bf16[4096,512]{1,0:T(8,128)(2,1)} %down_second.1), custom_call_target="tpu_custom_call" | custom-call | tf_op jit(solution)/shard_map/pallas_call | solution.py:554
  44.3 0.6 %copy.10 = bf16[64,512]{1,0:T(8,128)(2,1)} copy(bf16[64,512]{1,0:T(8,128)(2,1)S(1)} %shard_map.82) | data formatting | bytes 131072
